TPU v7x, 32 devices: a whole 2x2x4 slice. The times are simulated.
32 devices in a mesh: grp: 2 (over x), sp: 8 (over z, y), tp: 2 (over core).
Axes of the slice: x: 2, y: 2, z: 4, core: 2. Of those that a mesh axis runs over, the one named last changes fastest.
Arguments:
- probe_preactivation: bfloat16 [4096, 2048], P(('grp', 'sp'), 'tp'), parts along dimension 0, may hold values from -6 to 6
- retention_preactivation: bfloat16 [4096, 2048], P(('grp', 'sp'), 'tp'), parts along dimension 0, may hold values from -5 to 5.5
- source_entries: bfloat16 [4096, 2048], P(('grp', 'sp'), 'tp'), parts along dimension 0, may hold values from -6 to 6
- extra_log_retention: float32 [4096, 16], P(('grp', 'sp'), 'tp'), parts along dimension 0, may hold values from -1.39 to 0
- retention_slack: float32 [2048], P('tp'), as said below
- group_normalizer_gain: float32 [128], replicated, may hold values from 0.1 to 1.9
- readout_mapping_matrix: bfloat16 [2048, 2048], P('tp'), may hold values from -0.125 to 0.125
Outputs:
- mixed: bfloat16 [4096, 2048], P(('grp', 'sp', 'tp')), parts along dimension 0
There are 2 independent parts, one for each index of `grp`. A program takes and returns all parts, laid end to end along the dimension named above; an argument that names none is the same for every part. Nothing has to cross between parts.
Inputs may be any that keep to these rules, and one draw needn't show every extreme that they name: `retention_slack`: every entry is positive.
All inputs are finite; a program needn't handle non-finite values.
Results may differ from a plain program's by a relative error of at most 0.014.
Values may be sent and summed in bfloat16 or wider, within the bound.
A program may use at most 128 MiB of HBM per device.

v0:
```python
import jax
import jax.numpy as jnp
from jax import lax
from jax.sharding import PartitionSpec as P

SPAN = 128


def carried_in(x, axis, join, neutral):
    place = lax.axis_index(axis)
    gathered = jax.tree.map(
        lambda a, kind: lax.all_gather(a.astype(kind), axis), x, (jnp.bfloat16, jnp.bfloat16)
    )
    state = jax.tree.map(lambda a, e: jnp.zeros_like(a) + jnp.asarray(e, a.dtype), x, neutral)

    def one(lap, state):
        return join(
            state,
            jax.tree.map(
                lambda a, own: lax.dynamic_index_in_dim(a, lap, 0, False).astype(own.dtype),
                gathered,
                x,
            ),
        )

    return lax.fori_loop(0, place, one, state)


def assemble_arguments(
    probe_preactivation,
    retention_preactivation,
    source_entries,
    extra_log_retention,
    retention_slack,
):
    tokens_here = probe_preactivation.shape[0]
    group_count = extra_log_retention.shape[1]
    head_dim = probe_preactivation.shape[1] // group_count
    probe_matrix = jax.nn.silu(probe_preactivation.astype(jnp.float32)).reshape(
        tokens_here, group_count, head_dim
    )
    scaled_address_matrix = (
        retention_slack * jax.nn.sigmoid(-retention_preactivation.astype(jnp.float32))
    ).reshape(tokens_here, group_count, head_dim)
    log_retention_factor = jnp.log1p(-scaled_address_matrix) + extra_log_retention[:, :, None]
    content_matrix = source_entries.reshape(tokens_here, group_count, head_dim)
    return (probe_matrix, scaled_address_matrix, content_matrix, log_retention_factor)


def advance(carried_state, scaled_address_matrix, content_matrix, running):
    final_running_sum = running[-1]
    passed_state = (scaled_address_matrix * jnp.exp(final_running_sum[None] - running)).astype(
        jnp.bfloat16
    )
    return jnp.exp(final_running_sum)[:, :, None] * carried_state + jnp.einsum(
        "wcf,wcz->cfz", passed_state, content_matrix, preferred_element_type=jnp.float32
    )


def block_pass(carried_state, pieces):
    probe_matrix, scaled_address_matrix, content_matrix, log_retention_factor = pieces
    span_len = probe_matrix.shape[0]
    running = jnp.cumsum(log_retention_factor, axis=0)
    raised_values = (probe_matrix * jnp.exp(running)).astype(jnp.bfloat16)
    lowered = (scaled_address_matrix * jnp.exp(-running)).astype(jnp.bfloat16)
    scores = jnp.einsum("thk,shk->hts", raised_values, lowered, preferred_element_type=jnp.float32)
    row_index = lax.broadcasted_iota(jnp.int32, (span_len, span_len), 0)
    col_index = lax.broadcasted_iota(jnp.int32, (span_len, span_len), 1)
    scores = jnp.where((row_index >= col_index)[None], scores, jnp.zeros_like(scores)).astype(
        jnp.bfloat16
    )
    final_output = jnp.einsum(
        "hts,shv->thv", scores, content_matrix, preferred_element_type=jnp.float32
    )
    final_output = final_output + jnp.einsum(
        "csq,sqd->csd",
        raised_values,
        carried_state.astype(jnp.bfloat16),
        preferred_element_type=jnp.float32,
    )
    carried_state = advance(carried_state, scaled_address_matrix, content_matrix, running)
    return (carried_state, (final_output, running))


def finish(mixer_out, group_normalizer_gain):
    scale = lax.rsqrt(jnp.mean(mixer_out * mixer_out, axis=-1, keepdims=True) + 1e-06)
    normed = (mixer_out * scale * group_normalizer_gain).astype(jnp.bfloat16)
    return normed.reshape(mixer_out.shape[0], mixer_out.shape[1] * mixer_out.shape[2])


def combine(earlier, later):
    return (earlier[0] * later[0], later[0][:, :, None] * earlier[1] + later[1])


def hand_along(totals, local_state):
    neutral = (jnp.ones_like(totals), jnp.zeros_like(local_state))
    return carried_in((totals, local_state), "sp", combine, neutral)[1]


def body(
    probe_preactivation,
    retention_preactivation,
    source_entries,
    extra_log_retention,
    retention_slack,
    group_normalizer_gain,
    readout_mapping_matrix,
):
    probe_matrix, scaled_address_matrix, content_matrix, log_retention_factor = assemble_arguments(
        probe_preactivation,
        retention_preactivation,
        source_entries,
        extra_log_retention,
        retention_slack,
    )
    tokens_here, group_count, head_dim = probe_matrix.shape
    blocks = tokens_here // SPAN
    pieces = tuple(
        (
            a.reshape(blocks, SPAN, group_count, head_dim)
            for a in (probe_matrix, scaled_address_matrix, content_matrix, log_retention_factor)
        )
    )
    empty = jnp.zeros((group_count, head_dim, head_dim), jnp.float32)
    zero_rate = jnp.zeros((group_count, head_dim), jnp.float32)

    def state_step(carry, piece):
        carried_state, offset = carry
        running = jnp.cumsum(piece[3], axis=0)
        carried_state = advance(carried_state, piece[1], piece[2], running)
        return ((carried_state, offset + running[-1]), None)

    (local_state, offset), _ = lax.scan(state_step, (empty, zero_rate), pieces)
    incoming = hand_along(jnp.exp(offset), local_state)
    _, (mixer_out, _) = lax.scan(block_pass, incoming, pieces)
    mixer_out = mixer_out.reshape(tokens_here, group_count, head_dim)
    normed = finish(mixer_out, group_normalizer_gain)
    return lax.psum_scatter(
        jnp.dot(normed, readout_mapping_matrix, preferred_element_type=jnp.float32).astype(
            jnp.bfloat16
        ),
        "tp",
        scatter_dimension=0,
        tiled=True,
    )


def solution(mesh):
    return jax.shard_map(
        body,
        mesh=mesh,
        in_specs=(
            P(("grp", "sp"), "tp"),
            P(("grp", "sp"), "tp"),
            P(("grp", "sp"), "tp"),
            P(("grp", "sp"), "tp"),
            P("tp"),
            P(),
            P("tp", None),
        ),
        out_specs=P(("grp", "sp", "tp"), None),
        check_vma=False,
    )
```

profile of v0, /device:TPU:27, one launch (start us, length us, event | category | flops | bytes accessed | tf_op | source)
XLA Modules:
  0.0 107.0 jit_solution(1581868485433337737)
XLA Ops:
  7.4 1.3 %multiply_bitcast_fusion = f32[32,8,8,128]{3,1,2,0:T(8,128)S(1)} fusion(bf16[256,1024]{1,0:T(8,128)(2,1)} %param.14, f32[1024]{0:T(1024)} %param.17), kind=kLoop, calls=%fused_computation.64 | loop fusion | flops 1048576 | bytes 1576960
  10.2 1.4 %log-plus-one_add_fusion = f32[2,128,8,128]{3,2,1,0:T(8,128)} fusion(f32[2,128,8]{2,1,0:T(8,128)S(1)} %copy.41, f32[2,128,8,128]{3,2,1,0:T(8,128)S(1)} %bitcast.125), kind=kLoop, calls=%fused_computation.63 | loop fusion | flops 524288 | bytes 2105344 | tf_op jit(solution)/shard_map/add | solution.py:45
  11.5 3.5 %while.39 = (s32[]{:T(128)}, f32[8,128,128]{2,1,0:T(8,128)S(1)}, f32[8,128]{1,0:T(8,128)S(1)}, f32[2,128,8,128]{3,2,1,0:T(8,128)}, f32[2,128,8,128]{3,2,1,0:T(8,...) while((s32[]{:T(128)}, f32[8,128,128]{2,1,0:T(8,128)S(1)}, ...), condition=%wide.region_2.3_spmd.clone, body=%wide.region_0.2_spmd.clone.sunk | while | flops 50989056 | bytes 3965044 | solution.py:133
  11.5 1.2 %fusion.79 = f32[128,8,128]{2,1,0:T(8,128)S(1)} fusion(f32[2,128,8,128]{3,2,1,0:T(8,128)} %get-tuple-element.365, s32[]{:T(128)S(6)} %copy.83), kind=kOutput, calls=%fused_computation.40.clone.1 | output fusion | flops 16646144 | bytes 1048580 | tf_op jit(solution)/shard_map/while/body/eval_jaxpr/jit(cumsum)/reduce_window_sum | solution.py:129
  13.3 1.2 %fusion.79 = f32[128,8,128]{2,1,0:T(8,128)S(1)} fusion(f32[2,128,8,128]{3,2,1,0:T(8,128)} %get-tuple-element.365, s32[]{:T(128)S(6)} %copy.83), kind=kOutput, calls=%fused_computation.40.clone.1 | output fusion | flops 16646144 | bytes 1048580 | tf_op jit(solution)/shard_map/while/body/eval_jaxpr/jit(cumsum)/reduce_window_sum | solution.py:129
  17.3 19.0 %all-gather = bf16[64,128]{1,0:T(8,128)(2,1)S(1)} all-gather(bf16[8,128]{1,0:T(8,128)(2,1)S(1)} %exponential_convert_fusion), channel_id=2, replica_groups=mesh['grp'=2,'sp'=8,'tp'=2] {'sp'}, dimensions={0}, use_global_device_ids=true | all-gather | bytes 18432 | tf_op jit(solution)/shard_map/all_gather | solution.py:12
  36.4 27.8 %all-gather.4.cloned.1.call-done = bf16[64,128,128]{2,1,0:T(8,128)(2,1)} async-done(((bf16[8,128,128]{2,1,0:T(8,128)(2,1)}), bf16[64,128,128]{2,1,0:T(8,128)(2,1)}) %all-gather.4.cloned.1.call-update) | async-done | bytes 2097168 | tf_op jit(solution)/shard_map/all_gather | solution.py:12
  64.3 7.7 %while.37 = (s32[]{:T(128)}, f32[8,128,128]{2,1,0:T(8,128)S(1)}, s32[]{:T(128)}, bf16[8,8,128]{2,1,0:T(8,128)(2,1)S(1)}, bf16[8,8,128,128]{3,2,1,0:T(8,128)(2,1)}, /*index=5*/s32[]{:T(128)}, s32[]{:T(128)}, s32[]{:T(128)}) while((s32[]{:T(128)}, f32[8,128,128]{2,1,0:T(8,128)S(1)}, s32[]{:T(128)}, bf16[8,8,128]{2,1,0:T(8,128)(2,1)S(1)}, ...), condition=%wide.region_4.5_spmd, body=%wide.region_3.4_spmd.sunk | while | flops 394245 | bytes 1321095 | solution.py:26
  64.3 1.2 %convert_add_fusion.2 = f32[8,128,128]{2,1,0:T(8,128)S(1)} fusion(f32[8,128,128]{2,1,0:T(8,128)S(1)} %get-tuple-element.379, bf16[8,8,128,128]{3,2,1,0:T(8,128)(2,1)} %get-tuple-element.390, s32[]{:T(128)S(6)} %select_n.18, f32[8,128]{1,0:T(8,128)S(1)} %bitcast_convert_fusion.2), kind=kLoop, calls=%fused_computation.clone.1 | loop fusion | flops 393216 | bytes 1314820 | tf_op jit(solution)/shard_map/while/body/add | solution.py:92
  65.6 1.2 %convert_add_fusion.2 = f32[8,128,128]{2,1,0:T(8,128)S(1)} fusion(f32[8,128,128]{2,1,0:T(8,128)S(1)} %get-tuple-element.379, bf16[8,8,128,128]{3,2,1,0:T(8,128)(2,1)} %get-tuple-element.390, s32[]{:T(128)S(6)} %select_n.18, f32[8,128]{1,0:T(8,128)S(1)} %bitcast_convert_fusion.2), kind=kLoop, calls=%fused_computation.clone.1 | loop fusion | flops 393216 | bytes 1314820 | tf_op jit(solution)/shard_map/while/body/add | solution.py:92
  66.9 1.2 %convert_add_fusion.2 = f32[8,128,128]{2,1,0:T(8,128)S(1)} fusion(f32[8,128,128]{2,1,0:T(8,128)S(1)} %get-tuple-element.379, bf16[8,8,128,128]{3,2,1,0:T(8,128)(2,1)} %get-tuple-element.390, s32[]{:T(128)S(6)} %select_n.18, f32[8,128]{1,0:T(8,128)S(1)} %bitcast_convert_fusion.2), kind=kLoop, calls=%fused_computation.clone.1 | loop fusion | flops 393216 | bytes 1314820 | tf_op jit(solution)/shard_map/while/body/add | solution.py:92
  68.1 1.2 %convert_add_fusion.2 = f32[8,128,128]{2,1,0:T(8,128)S(1)} fusion(f32[8,128,128]{2,1,0:T(8,128)S(1)} %get-tuple-element.379, bf16[8,8,128,128]{3,2,1,0:T(8,128)(2,1)} %get-tuple-element.390, s32[]{:T(128)S(6)} %select_n.18, f32[8,128]{1,0:T(8,128)S(1)} %bitcast_convert_fusion.2), kind=kLoop, calls=%fused_computation.clone.1 | loop fusion | flops 393216 | bytes 1314820 | tf_op jit(solution)/shard_map/while/body/add | solution.py:92
  69.4 1.2 %convert_add_fusion.2 = f32[8,128,128]{2,1,0:T(8,128)S(1)} fusion(f32[8,128,128]{2,1,0:T(8,128)S(1)} %get-tuple-element.379, bf16[8,8,128,128]{3,2,1,0:T(8,128)(2,1)} %get-tuple-element.390, s32[]{:T(128)S(6)} %select_n.18, f32[8,128]{1,0:T(8,128)S(1)} %bitcast_convert_fusion.2), kind=kLoop, calls=%fused_computation.clone.1 | loop fusion | flops 393216 | bytes 1314820 | tf_op jit(solution)/shard_map/while/body/add | solution.py:92
  70.7 1.2 %convert_add_fusion.2 = f32[8,128,128]{2,1,0:T(8,128)S(1)} fusion(f32[8,128,128]{2,1,0:T(8,128)S(1)} %get-tuple-element.379, bf16[8,8,128,128]{3,2,1,0:T(8,128)(2,1)} %get-tuple-element.390, s32[]{:T(128)S(6)} %select_n.18, f32[8,128]{1,0:T(8,128)S(1)} %bitcast_convert_fusion.2), kind=kLoop, calls=%fused_computation.clone.1 | loop fusion | flops 393216 | bytes 1314820 | tf_op jit(solution)/shard_map/while/body/add | solution.py:92
  71.9 9.1 %while.38 = (s32[]{:T(128)}, f32[8,128,128]{2,1,0:T(8,128)S(1)}, f32[2,128,8,128]{1,3,2,0:T(8,128)}, f32[2,128,8,128]{3,2,1,0:T(8,128)}, f32[2,128,8,128]{3,2,1,...) while((s32[]{:T(128)}, f32[8,128,128]{2,1,0:T(8,128)S(1)}, ...), condition=%wide.region_7.8_spmd, body=%wide.region_5.7_spmd.sunk | while | flops 152715264 | bytes 8184937 | solution.py:135
  71.9 1.2 %fusion.72 = f32[128,8,128]{2,1,0:T(8,128)S(1)} fusion(f32[2,128,8,128]{3,2,1,0:T(8,128)} %get-tuple-element.413, s32[]{:T(128)S(6)} %copy.98), kind=kOutput, calls=%fused_computation.16.clone.1 | output fusion | flops 16646144 | bytes 1048580 | tf_op jit(solution)/shard_map/while/body/eval_jaxpr/jit(cumsum)/reduce_window_sum | solution.py:63
  73.1 1.3 %fusion.73 = (bf16[128,8,128]{2,1,0:T(8,128)(2,1)S(1)}, bf16[128,8,128]{2,1,0:T(8,128)(2,1)S(1)}, bf16[128,8,128]{2,1,0:T(8,128)(2,1)S(1)}) fusion(f32[128,8,128]{2,1,0:T(8,128)S(1)} %fusion.72, f32[2,128,8,128]{3,2,1,0:T(8,128)S(1)} %get-tuple-element.414, s32[]{:T(128)S(6)} %copy.98, f32[8,128]{1,0:T(8,128)S(1)} %slice_bitcast_fusion.4, ...), kind=kLoop, calls=%fused_computation.15.clone.1 | loop fusion | flops 1048576 | bytes 2363396 | tf_op jit(solution)/shard_map/while/body/eval_jaxpr/convert_element_type | solution.py:65
  75.2 1.3 %fusion.75 = f32[2,128,8,128]{1,3,2,0:T(8,128)} fusion(f32[2,128,8,128]{1,3,2,0:T(8,128)} %get-tuple-element.404, s32[]{:T(128)S(6)} %copy.98, f32[128,8,128]{0,2,1:T(8,128)S(1)} %convolution_bitcast_fusion.3, bf16[128,8,128]{2,1,0:T(8,128)(2,1)S(1)} %get-tuple-element.337, pred[128,128]{1,0:T(8,128)(4,1)S(1)} %iota_compare_fusion.2, ...), kind=kOutput, calls=%fused_computation.7.clone.1 | convolution fusion | flops 67502080 | bytes 1852416 | tf_op jit(solution)/shard_map/while/body/eval_jaxpr/hts,shv->thv/dot_general | solution.py:72
  77.7 1.3 %fusion.73 = (bf16[128,8,128]{2,1,0:T(8,128)(2,1)S(1)}, bf16[128,8,128]{2,1,0:T(8,128)(2,1)S(1)}, bf16[128,8,128]{2,1,0:T(8,128)(2,1)S(1)}) fusion(f32[128,8,128]{2,1,0:T(8,128)S(1)} %fusion.72, f32[2,128,8,128]{3,2,1,0:T(8,128)S(1)} %get-tuple-element.414, s32[]{:T(128)S(6)} %copy.98, f32[8,128]{1,0:T(8,128)S(1)} %slice_bitcast_fusion.4, ...), kind=kLoop, calls=%fused_computation.15.clone.1 | loop fusion | flops 1048576 | bytes 2363396 | tf_op jit(solution)/shard_map/while/body/eval_jaxpr/convert_element_type | solution.py:65
  79.8 1.3 %fusion.75 = f32[2,128,8,128]{1,3,2,0:T(8,128)} fusion(f32[2,128,8,128]{1,3,2,0:T(8,128)} %get-tuple-element.404, s32[]{:T(128)S(6)} %copy.98, f32[128,8,128]{0,2,1:T(8,128)S(1)} %convolution_bitcast_fusion.3, bf16[128,8,128]{2,1,0:T(8,128)(2,1)S(1)} %get-tuple-element.337, pred[128,128]{1,0:T(8,128)(4,1)S(1)} %iota_compare_fusion.2, ...), kind=kOutput, calls=%fused_computation.7.clone.1 | convolution fusion | flops 67502080 | bytes 1852416 | tf_op jit(solution)/shard_map/while/body/eval_jaxpr/hts,shv->thv/dot_general | solution.py:72
  81.1 1.3 %multiply_reduce_fusion = f32[2,128,8]{1,2,0:T(8,128)S(1)} fusion(f32[2,128,8,128]{1,3,2,0:T(8,128)} %get-tuple-element.122), kind=kLoop, calls=%fused_computation.62 | loop fusion | flops 522240 | bytes 1056768 | tf_op jit(solution)/shard_map/reduce_sum | solution.py:86
  82.4 1.6 %copy.44 = f32[2,128,8,128]{3,2,1,0:T(8,128)S(1)} copy(f32[2,128,8,128]{1,3,2,0:T(8,128)} %get-tuple-element.122) | data formatting | bytes 2097152 | tf_op jit(solution)/shard_map/while | solution.py:135
  84.5 4.6 %convolution_convert_fusion = bf16[256,2048]{1,0:T(8,128)(2,1)} fusion(bf16[1024,2048]{1,0:T(8,128)(2,1)} %param.19, f32[32,8,8,128]{3,2,1,0:T(8,128)S(1)} %bitcast.129, f32[32,8,8,128]{3,2,1,0:T(8,128)S(1)} %bitcast.130, f32[1024]{0:T(1024)S(1)} %broadcast_bitcast_fusion), kind=kOutput, calls=%fused_computation.52 | convolution fusion | flops 1075052544 | bytes 7344128 | tf_op jit(solution)/shard_map/dot_general | solution.py:139
  89.1 11.1 %reduce-scatter.2.cloned.1.call-done = bf16[128,2048]{1,0:T(8,128)(2,1)} async-done(((bf16[256,2048]{1,0:T(8,128)(2,1)}), bf16[128,2048]{1,0:T(8,128)(2,1)}) %reduce-scatter.2.cloned.1.call-update) | async-done | bytes 524304 | tf_op jit(solution)/shard_map/reduce_scatter | solution.py:138
  (49 shorter events, 8.8 us)
Async XLA Ops:
  6.5 29.8 %copy-start = (f32[128]{0:T(128)S(1)}, f32[128]{0:T(128)}, u32[]{:S(2)}) copy-start(f32[128]{0:T(128)} %param.18) | copy-start | bytes 1540
  6.5 57.7 %all-gather.4.cloned.1.call-start = ((), (), s32[]{:S(2)}) async-start(), calls=%async_computation.2 | async-start | bytes 2359296 | tf_op jit(solution)/shard_map/all_gather | solution.py:12
  11.5 4.3 %copy-start.1 = (bf16[256,1024]{1,0:T(8,128)(2,1)S(1)}, bf16[256,1024]{1,0:T(8,128)(2,1)}, u32[]{:S(2)}) copy-start(bf16[256,1024]{1,0:T(8,128)(2,1)} %param.13) | copy-start | bytes 1572868
  15.8 84.4 %reduce-scatter.2.cloned.1.call-start = ((), (), s32[]{:S(2)}) async-start(), calls=%async_computation.1 | async-start | bytes 1572864 | tf_op jit(solution)/shard_map/reduce_scatter | solution.py:138
Sparse Core Ops, SparseCore 0:
  15.9 48.2 all-gather.3
  89.2 10.9 reduce-scatter.1
where the time goes:
time: 109 us; the launch traced here: 107 us
  waiting for transfers between devices  39 us (36%)
  other arithmetic  20.1 us (18%)
  blocking collectives  19 us (17%)
  between operations  13.5 us (12%)
  matrix products  9.43 us (9%)
  local copies, waits for them, and re-layouts  5.56 us (5%)
    all_gather x1, waiting for transfers between devices, carried_in(): lax.all_gather(a.astype(kind), axis)  27.8 us
    all_gather x1, blocking collectives, carried_in(): lax.all_gather(a.astype(kind), axis)  19 us
    reduce_scatter x1, waiting for transfers between devices, body(): lax.psum_scatter(jnp.dot(normed, readout_mapping_matrix, preferred_elemen...  11.1 us
    add x6, other arithmetic, combine(): return (earlier[0] * later[0], later[0][:, :, None] * earlier[1] + later[1])  7.38 us
    dot_general x1, matrix products, body(): jnp.dot(normed, readout_mapping_matrix, preferred_element_type=jnp.float32)  4.56 us
    unnamed x8, local copies, waits for them, and re-layouts  2.61 us
    dot_general x2, matrix products, block_pass(): jnp.einsum('hts,shv->thv', scores, content_matrix, preferred_element_type...  2.6 us
    convert_element_type x2, other arithmetic, block_pass(): lowered = (scaled_address_matrix * jnp.exp(-running)).astype(jnp.bfloat16)  2.58 us
  transfers between devices with their start and end apart: 2, of which 2 were waited for; matrix products, arithmetic and copies ran while one was open for 1% of the time, Pallas kernels for 0%

commit v1 on v0

v1 whole, which is shorter than its diff:
```python
import functools

import jax
import jax.numpy as jnp
from jax import lax
from jax.experimental import pallas as pl
from jax.experimental.pallas import tpu as pltpu
from jax.sharding import PartitionSpec as P

SPAN = 128
GROUP = 2
TILES = 4
MESH = pl.DeviceIdType.MESH
F32 = jnp.float32
BF16 = jnp.bfloat16


def dot(a, b, contract):
    return lax.dot_general(a, b, (contract, ((), ())), preferred_element_type=F32)


def kernel(
    n_sp,
    p_hbm,
    r_hbm,
    v_hbm,
    x_ref,
    slack_ref,
    gain_ref,
    w_hbm,
    out_ref,
    p_ref,
    r_ref,
    v_ref,
    w_ref,
    lifted,
    lowered,
    lfull,
    inner,
    local,
    decay,
    intra,
    swap_out,
    swap_in,
    chain_out,
    chain_in,
    enter,
    normed,
    acc,
    half_out,
    half_in,
    in_sem,
    w_sem,
    swap_send,
    swap_recv,
    chain_send,
    chain_recv,
    half_send,
    half_recv,
):
    tokens, channels = p_ref.shape
    heads = x_ref.shape[0]
    dim = channels // heads
    blocks = tokens // SPAN
    groups = heads // GROUP
    wide = w_ref.shape[1]
    tile = wide // TILES
    half = out_ref.shape[0]
    sp, tp = lax.axis_index("sp"), lax.axis_index("tp")
    pairs = n_sp // 2
    pair, odd = sp // 2, sp % 2
    mate = sp + 1 - 2 * odd
    first, last = pair == 0, pair == pairs - 1

    loads = []
    for g in range(groups):
        cols = pl.ds(g * GROUP * dim, GROUP * dim)
        loads.append(
            [
                pltpu.make_async_copy(src.at[:, cols], dst.at[:, cols], in_sem.at[g, i])
                for i, (src, dst) in enumerate(((r_hbm, r_ref), (v_hbm, v_ref), (p_hbm, p_ref)))
            ]
        )
        for c in loads[g]:
            c.start()
    w_loads = []
    for g in range(groups):
        rows = pl.ds(g * GROUP * dim, GROUP * dim)
        w_loads.append(pltpu.make_async_copy(w_hbm.at[rows, :], w_ref.at[rows, :], w_sem.at[g]))
        w_loads[g].start()

    barrier = pltpu.get_barrier_semaphore()
    pl.semaphore_signal(barrier, inc=1, device_id={"sp": mate}, device_id_type=MESH)
    pl.semaphore_signal(barrier, inc=1, device_id={"tp": 1 - tp}, device_id_type=MESH)

    @pl.when(jnp.logical_not(first))
    def _():
        pl.semaphore_signal(barrier, inc=1, device_id={"sp": sp - 2}, device_id_type=MESH)

    @pl.when(jnp.logical_not(last))
    def _():
        pl.semaphore_signal(barrier, inc=1, device_id={"sp": sp + 2}, device_id_type=MESH)

    @pl.when(first)
    def _():
        chain_in[...] = jnp.zeros_like(chain_in)

    extra = x_ref[...].T
    row = lax.broadcasted_iota(jnp.int32, (SPAN, SPAN), 0)
    col = lax.broadcasted_iota(jnp.int32, (SPAN, SPAN), 1)
    causal = row >= col
    tri = jnp.where(causal, 1.0, 0.0).astype(BF16)
    tri2 = jnp.concatenate([tri, tri], axis=1)
    tag = lax.broadcasted_iota(jnp.int32, (16, dim), 0) == 0

    def swap(h):
        return pltpu.make_async_remote_copy(
            swap_out.at[h],
            swap_in.at[h],
            swap_send.at[h],
            swap_recv.at[h],
            device_id={"sp": mate},
            device_id_type=MESH,
        )

    def chain(h):
        return pltpu.make_async_remote_copy(
            chain_out.at[h],
            chain_in.at[h],
            chain_send.at[h],
            chain_recv.at[h],
            device_id={"sp": jnp.minimum(sp + 2, n_sp - 2 + odd)},
            device_id_type=MESH,
        )

    def summarise(h):
        hs = slice(h * dim, (h + 1) * dim)
        slack = slack_ref[:, hs]
        state, offset = None, None
        for b in range(blocks):
            ts = slice(b * SPAN, (b + 1) * SPAN)
            keyed = slack * (0.5 - 0.5 * jnp.tanh(0.5 * r_ref[ts, hs].astype(F32)))
            log_decay = jnp.log(1.0 - keyed) + extra[ts, h : h + 1]
            high = log_decay.astype(BF16)
            low = (log_decay - high.astype(F32)).astype(BF16)
            running = dot(tri2, jnp.concatenate([high, low], axis=0), ((1,), (0,)))
            end = running[SPAN - 1 :, :]
            probe = p_ref[ts, hs].astype(F32)
            query = probe * (0.5 + 0.5 * jnp.tanh(0.5 * probe))
            raised = query * jnp.exp(running)
            lifted[ts, hs] = raised.astype(BF16)
            lowered[ts, hs] = (keyed * jnp.exp(-running)).astype(BF16)
            sent = (keyed * jnp.exp(end - running)).astype(BF16)
            fresh = dot(v_ref[ts, hs], sent, ((0,), (0,)))
            if b == 0:
                lfull[ts, hs] = raised.astype(BF16)
                state, offset = fresh, end
            else:
                lfull[ts, hs] = (raised * jnp.exp(offset)).astype(BF16)
                inner[h, b - 1] = state.astype(BF16)
                state, offset = jnp.exp(end) * state + fresh, offset + end
        local[h] = state
        total = jnp.exp(offset)
        decay[h] = jnp.broadcast_to(total, (8, dim))
        high = total.astype(BF16)
        low = (total - high.astype(F32)).astype(BF16)
        swap_out[h, :dim, :] = state.astype(BF16)
        swap_out[h, dim:, :] = jnp.where(tag, high.astype(F32), low.astype(F32)).astype(BF16)

    def pass_on(h):
        swap(h).wait_recv()
        other = swap_in[h, :dim, :].astype(F32)
        tail = swap_in[h, dim:, :].astype(F32)
        d_other = tail[0:1] + tail[1:2]
        own, d_own = local[h], decay[h, 0:1, :]
        is_odd = odd == 1
        s0 = jnp.where(is_odd, other, own)
        s1 = jnp.where(is_odd, own, other)
        d0 = jnp.where(is_odd, d_other, d_own)
        d1 = jnp.where(is_odd, d_own, d_other)
        before = chain_in[h].astype(F32)
        middle = d0 * before + s0
        chain_out[h] = (d1 * middle + s1).astype(BF16)

        @pl.when(jnp.logical_not(last))
        def _():
            chain(h).start()

        enter[h] = jnp.where(is_odd, middle, before).astype(BF16)

    def within(h):
        hs = slice(h * dim, (h + 1) * dim)
        for b in range(blocks):
            ts = slice(b * SPAN, (b + 1) * SPAN)
            up = lifted[ts, hs]
            scores = dot(up, lowered[ts, hs], ((1,), (1,)))
            scores = jnp.where(causal, scores, 0.0).astype(BF16)
            o = dot(scores, v_ref[ts, hs], ((1,), (0,)))
            if b > 0:
                o = o + dot(up, inner[h, b - 1], ((1,), (1,)))
            intra[ts, hs] = o

    gain = gain_ref[...]

    def close(h):
        hs = slice(h * dim, (h + 1) * dim)
        o = intra[:, hs] + dot(lfull[:, hs], enter[h], ((1,), (1,)))
        scale = lax.rsqrt(jnp.mean(o * o, axis=-1, keepdims=True) + 1e-6)
        normed[:, hs] = (o * scale * gain).astype(BF16)

    for g in range(groups):
        for c in loads[g]:
            c.wait()
        for h in range(g * GROUP, (g + 1) * GROUP):
            summarise(h)
        if g == 0:
            pl.semaphore_wait(barrier, 4 - first.astype(jnp.int32) - last.astype(jnp.int32))

        for h in range(g * GROUP, (g + 1) * GROUP):
            swap(h).start()

    @pl.when(first)
    def _():
        for h in range(heads):
            pass_on(h)

    for h in range(heads):
        within(h)

    theirs = pl.ds(pl.multiple_of((1 - tp) * half, half), half)
    mine = pl.ds(pl.multiple_of(tp * half, half), half)

    def exchange(t):
        ns = pl.ds(t * tile, tile)
        return pltpu.make_async_remote_copy(
            half_out.at[:, ns],
            half_in.at[:, ns],
            half_send.at[t],
            half_recv.at[t],
            device_id={"tp": 1 - tp},
            device_id_type=MESH,
        )

    for g in range(groups):
        hs = range(g * GROUP, (g + 1) * GROUP)

        @pl.when(jnp.logical_not(first))
        def _():
            for h in hs:
                chain(h).wait_recv()
                pass_on(h)

        for h in hs:
            close(h)
        w_loads[g].wait()
        ks = slice(g * GROUP * dim, (g + 1) * GROUP * dim)
        if g < groups - 1:
            for t in range(TILES):
                ns = slice(t * tile, (t + 1) * tile)
                part = dot(normed[:, ks], w_ref[ks, ns], ((1,), (0,)))
                acc[:, ns] = part if g == 0 else acc[:, ns] + part
        else:
            for t in range(TILES):
                ns = slice(t * tile, (t + 1) * tile)
                part = dot(normed[theirs, ks], w_ref[ks, ns], ((1,), (0,)))
                if groups > 1:
                    part = part + acc[theirs, ns]
                half_out[:, ns] = part.astype(BF16)
                exchange(t).start()
            for t in range(TILES):
                ns = slice(t * tile, (t + 1) * tile)
                part = dot(normed[mine, ks], w_ref[ks, ns], ((1,), (0,)))
                if groups > 1:
                    part = part + acc[mine, ns]
                exchange(t).wait_recv()
                out_ref[:, ns] = (part + half_in[:, ns].astype(F32)).astype(BF16)

    for h in range(heads):
        swap(h).wait_send()

    @pl.when(jnp.logical_not(last))
    def _():
        for h in range(heads):
            chain(h).wait_send()

    for t in range(TILES):
        exchange(t).wait_send()


def body(n_sp, n_tp, p, r, v, x, slack, gain, w):
    tokens, channels = p.shape
    heads = x.shape[1]
    dim = channels // heads
    blocks = tokens // SPAN
    groups = heads // GROUP
    wide = w.shape[1]
    half = tokens // n_tp
    vmem = pl.BlockSpec(memory_space=pltpu.VMEM)
    hbm = pl.BlockSpec(memory_space=pl.ANY)
    dma = pltpu.SemaphoreType.DMA
    return pl.pallas_call(
        functools.partial(kernel, n_sp),
        out_shape=jax.ShapeDtypeStruct((half, wide), BF16),
        in_specs=[hbm, hbm, hbm, vmem, vmem, vmem, hbm],
        out_specs=vmem,
        scratch_shapes=[
            pltpu.VMEM((tokens, channels), BF16),
            pltpu.VMEM((tokens, channels), BF16),
            pltpu.VMEM((tokens, channels), BF16),
            pltpu.VMEM(w.shape, BF16),
            pltpu.VMEM((tokens, channels), BF16),
            pltpu.VMEM((tokens, channels), BF16),
            pltpu.VMEM((tokens, channels), BF16),
            pltpu.VMEM((heads, max(blocks - 1, 1), dim, dim), BF16),
            pltpu.VMEM((heads, dim, dim), F32),
            pltpu.VMEM((heads, 8, dim), F32),
            pltpu.VMEM((tokens, channels), F32),
            pltpu.VMEM((heads, dim + 16, dim), BF16),
            pltpu.VMEM((heads, dim + 16, dim), BF16),
            pltpu.VMEM((heads, dim, dim), BF16),
            pltpu.VMEM((heads, dim, dim), BF16),
            pltpu.VMEM((heads, dim, dim), BF16),
            pltpu.VMEM((tokens, channels), BF16),
            pltpu.VMEM((tokens, wide), F32),
            pltpu.VMEM((half, wide), BF16),
            pltpu.VMEM((half, wide), BF16),
            dma((groups, 3)),
            dma((groups,)),
            dma((heads,)),
            dma((heads,)),
            dma((heads,)),
            dma((heads,)),
            dma((TILES,)),
            dma((TILES,)),
        ],
        compiler_params=pltpu.CompilerParams(
            collective_id=0, has_side_effects=True, vmem_limit_bytes=60 * 2**20
        ),
    )(p, r, v, x.T, slack.reshape(1, channels), gain.reshape(1, dim), w)


def solution(mesh):
    return jax.shard_map(
        functools.partial(body, mesh.shape["sp"], mesh.shape["tp"]),
        mesh=mesh,
        in_specs=(
            P(("grp", "sp"), "tp"),
            P(("grp", "sp"), "tp"),
            P(("grp", "sp"), "tp"),
            P(("grp", "sp"), "tp"),
            P("tp"),
            P(),
            P("tp", None),
        ),
        out_specs=P(("grp", "sp", "tp"), None),
        check_vma=False,
    )
```

time: 109 us -> 24.9 us (0.23); the launches traced: 107 us -> 24.7 us
  waiting for transfers between devices: 39 us -> 0 us
  Pallas kernels: 0 us -> 22.8 us
  other arithmetic: 20.1 us -> 0 us
  blocking collectives: 19 us -> 0 us
  between operations: 13.5 us -> 0.01 us
  matrix products: 9.43 us -> 0 us
  local copies, waits for them, and re-layouts: 5.56 us -> 1.88 us
    all_gather x1 -> x0, waiting for transfers between devices: 27.8 us -> none  [carried_in(): lax.all_gather(a.astype(kind), axis)]
    pallas_call x0 -> x1, Pallas kernels: none -> 22.8 us  [body(): pl.pallas_call(functools.partial(kernel, n_sp), out_shape=jax.ShapeDtypeS...]
    all_gather x1 -> x0, blocking collectives: 19 us -> none  [carried_in(): lax.all_gather(a.astype(kind), axis)]
    reduce_scatter x1 -> x0, waiting for transfers between devices: 11.1 us -> none  [body(): lax.psum_scatter(jnp.dot(normed, readout_mapping_matrix, preferred_elemen...]
    dot_general x9 -> x0, matrix products: 9.43 us -> none  [the longest x1 4.56 us: body(): jnp.dot(normed, readout_mapping_matrix, preferred_element_type=jnp.float32)]
    add x9 -> x0, other arithmetic: 8.77 us -> none  [the longest x6 7.38 us: combine(): return (earlier[0] * later[0], later[0][:, :, None] * earlier[1] + later[1])]
    another operation x4 -> x0, other arithmetic: 4.77 us -> none  [the longest x2 2.42 us: state_step(): running = jnp.cumsum(piece[3], axis=0)]
    convert_element_type x12 -> x0, other arithmetic: 3.6 us -> none  [the longest x2 2.58 us: block_pass(): lowered = (scaled_address_matrix * jnp.exp(-running)).astype(jnp.bfloat16)]
  transfers between devices with their start and end apart: 2 -> 0, of which waited for: 2 -> 0; matrix products, arithmetic and copies ran while one was open for 1% -> 0% of each run, Pallas kernels for 0% -> 0%
where the time goes in v1:
time: 24.9 us; the launch traced here: 24.7 us
  Pallas kernels  22.8 us (92%)
  local copies, waits for them, and re-layouts  1.88 us (8%)
    pallas_call x1, Pallas kernels, body(): pl.pallas_call(functools.partial(kernel, n_sp), out_shape=jax.ShapeDtypeS...  22.8 us
    unnamed x1, local copies, waits for them, and re-layouts  1.88 us

profile of v1, /device:TPU:27, one launch (start us, length us, event | category | flops | bytes accessed | tf_op | source)
XLA Modules:
  0.0 24.7 jit_solution(1517066624322320527)
XLA Ops:
  0.0 22.8 %shard_map.73 = bf16[128,2048]{1,0:T(8,128)(2,1)} custom-call(bf16[256,1024]{1,0:T(8,128)(2,1)} %p_hbm.1, bf16[256,1024]{1,0:T(8,128)(2,1)} %r_hbm.1, bf16[256,1024]{1,0:T(8,128)(2,1)} %v_hbm.1, f32[8,256]{1,0:T(8,128)} %bitcast.3, f32[1,1024]{1,0:T(1,128)} %bitcast.4, f32[1,128]{1,0:T(1,128)} %bitcast.5, bf16[1024,2048]{1,0:T(8,128)(2,1)} %w_hbm.1), custom_call_target="tpu_custom_call" | custom-call | tf_op jit(solution)/shard_map/pallas_call | solution.py:301
  22.8 1.9 %copy.9 = bf16[128,2048]{1,0:T(8,128)(2,1)} copy(bf16[128,2048]{1,0:T(8,128)(2,1)} %shard_map.73) | data formatting | bytes 1048576

commit v2 on v1

--- a/solution.py
+++ b/solution.py
@@ -10,6 +10,7 @@
 SPAN = 128
 GROUP = 2
 TILES = 4
+PIECES = 2
 MESH = pl.DeviceIdType.MESH
 F32 = jnp.float32
 BF16 = jnp.bfloat16
@@ -123,12 +124,13 @@
             device_id_type=MESH,
         )
 
-    def chain(h):
+    def chain(h, c):
+        rows = pl.ds(c * (dim // PIECES), dim // PIECES)
         return pltpu.make_async_remote_copy(
-            chain_out.at[h],
-            chain_in.at[h],
-            chain_send.at[h],
-            chain_recv.at[h],
+            chain_out.at[h, rows],
+            chain_in.at[h, rows],
+            chain_send.at[h, c],
+            chain_recv.at[h, c],
             device_id={"sp": jnp.minimum(sp + 2, n_sp - 2 + odd)},
             device_id_type=MESH,
         )
@@ -167,26 +169,29 @@
         swap_out[h, :dim, :] = state.astype(BF16)
         swap_out[h, dim:, :] = jnp.where(tag, high.astype(F32), low.astype(F32)).astype(BF16)
 
-    def pass_on(h):
+    def pass_on(h, arrival):
         swap(h).wait_recv()
-        other = swap_in[h, :dim, :].astype(F32)
         tail = swap_in[h, dim:, :].astype(F32)
-        d_other = tail[0:1] + tail[1:2]
-        own, d_own = local[h], decay[h, 0:1, :]
+        d_other, d_own = tail[0:1] + tail[1:2], decay[h, 0:1, :]
         is_odd = odd == 1
-        s0 = jnp.where(is_odd, other, own)
-        s1 = jnp.where(is_odd, own, other)
         d0 = jnp.where(is_odd, d_other, d_own)
         d1 = jnp.where(is_odd, d_own, d_other)
-        before = chain_in[h].astype(F32)
-        middle = d0 * before + s0
-        chain_out[h] = (d1 * middle + s1).astype(BF16)
-
-        @pl.when(jnp.logical_not(last))
-        def _():
-            chain(h).start()
-
-        enter[h] = jnp.where(is_odd, middle, before).astype(BF16)
+        for c in range(PIECES):
+            rows = pl.ds(c * (dim // PIECES), dim // PIECES)
+            other, own = swap_in[h, rows, :].astype(F32), local[h, rows, :]
+            s0 = jnp.where(is_odd, other, own)
+            s1 = jnp.where(is_odd, own, other)
+            if arrival:
+                chain(h, c).wait_recv()
+            before = chain_in[h, rows, :].astype(F32)
+            middle = d0 * before + s0
+            chain_out[h, rows, :] = (d1 * middle + s1).astype(BF16)
+
+            @pl.when(jnp.logical_not(last))
+            def _():
+                chain(h, c).start()
+
+            enter[h, rows, :] = jnp.where(is_odd, middle, before).astype(BF16)
 
     def within(h):
         hs = slice(h * dim, (h + 1) * dim)
@@ -219,13 +224,12 @@
         for h in range(g * GROUP, (g + 1) * GROUP):
             swap(h).start()
 
-    @pl.when(first)
-    def _():
-        for h in range(heads):
-            pass_on(h)
-
     for h in range(heads):
         within(h)
+
+        @pl.when(first)
+        def _():
+            pass_on(h, False)
 
     theirs = pl.ds(pl.multiple_of((1 - tp) * half, half), half)
     mine = pl.ds(pl.multiple_of(tp * half, half), half)
@@ -244,11 +248,17 @@
     for g in range(groups):
         hs = range(g * GROUP, (g + 1) * GROUP)
 
-        @pl.when(jnp.logical_not(first))
+        ahead = range(0 if g == 0 else (g + 1) * GROUP, min(g + 2, groups) * GROUP)
+
+        @pl.when(jnp.logical_and(jnp.logical_not(first), jnp.logical_not(last)))
+        def _():
+            for h in ahead:
+                pass_on(h, True)
+
+        @pl.when(jnp.logical_and(jnp.logical_not(first), last))
         def _():
             for h in hs:
-                chain(h).wait_recv()
-                pass_on(h)
+                pass_on(h, True)
 
         for h in hs:
             close(h)
@@ -281,7 +291,8 @@
     @pl.when(jnp.logical_not(last))
     def _():
         for h in range(heads):
-            chain(h).wait_send()
+            for c in range(PIECES):
+                chain(h, c).wait_send()
 
     for t in range(TILES):
         exchange(t).wait_send()
@@ -295,8 +306,12 @@
     groups = heads // GROUP
     wide = w.shape[1]
     half = tokens // n_tp
+    x, slack, gain = x.T, slack.reshape(1, channels), gain.reshape(1, dim)
+    p, r, v, x, slack, gain, w = (
+        pltpu.with_memory_space_constraint(a, pltpu.HBM) for a in (p, r, v, x, slack, gain, w)
+    )
     vmem = pl.BlockSpec(memory_space=pltpu.VMEM)
-    hbm = pl.BlockSpec(memory_space=pl.ANY)
+    hbm = pl.BlockSpec(memory_space=pltpu.HBM)
     dma = pltpu.SemaphoreType.DMA
     return pl.pallas_call(
         functools.partial(kernel, n_sp),
@@ -328,15 +343,15 @@
             dma((groups,)),
             dma((heads,)),
             dma((heads,)),
-            dma((heads,)),
-            dma((heads,)),
+            dma((heads, PIECES)),
+            dma((heads, PIECES)),
             dma((TILES,)),
             dma((TILES,)),
         ],
         compiler_params=pltpu.CompilerParams(
-            collective_id=0, has_side_effects=True, vmem_limit_bytes=60 * 2**20
+            collective_id=0, has_side_effects=True, vmem_limit_bytes=24 * 2**20
         ),
-    )(p, r, v, x.T, slack.reshape(1, channels), gain.reshape(1, dim), w)
+    )(p, r, v, x, slack, gain, w)
 
 
 def solution(mesh):

time: 24.9 us -> 22.9 us (0.920)
  local copies, waits for them, and re-layouts: 1.88 us -> 0.8 us
  Pallas kernels: 22.8 us -> 21.9 us
    unnamed x1, local copies, waits for them, and re-layouts: 1.88 us -> 0.8 us
    pallas_call x1, Pallas kernels: 22.8 us -> 21.9 us  [body(): pl.pallas_call(functools.partial(kernel, n_sp), out_shape=jax.ShapeDtypeS...]
where the time goes in v2:
time: 22.9 us; the launch traced here: 22.7 us
  Pallas kernels  21.9 us (96%)
  local copies, waits for them, and re-layouts  0.8 us (3%)
    pallas_call x1, Pallas kernels, body(): pl.pallas_call(functools.partial(kernel, n_sp), out_shape=jax.ShapeDtypeS...  21.9 us
    unnamed x1, local copies, waits for them, and re-layouts  0.8 us

profile of v2, /device:TPU:27, one launch (start us, length us, event | category | flops | bytes accessed | tf_op | source)
XLA Modules:
  0.0 22.7 jit_solution(17235909121996633178)
XLA Ops:
  0.0 21.9 %shard_map.73 = bf16[128,2048]{1,0:T(8,128)(2,1)S(1)} custom-call(bf16[256,1024]{1,0:T(8,128)(2,1)} %p_hbm.1, bf16[256,1024]{1,0:T(8,128)(2,1)} %r_hbm.1, bf16[256,1024]{1,0:T(8,128)(2,1)} %v_hbm.1, f32[8,256]{1,0:T(8,128)} %bitcast.3, f32[1,1024]{1,0:T(1,128)} %bitcast.4, f32[1,128]{1,0:T(1,128)} %bitcast.5, bf16[1024,2048]{1,0:T(8,128)(2,1)} %w_hbm.1), custom_call_target="tpu_custom_call" | custom-call | tf_op jit(solution)/shard_map/pallas_call | solution.py:316
  21.9 0.8 %copy.9 = bf16[128,2048]{1,0:T(8,128)(2,1)} copy(bf16[128,2048]{1,0:T(8,128)(2,1)S(1)} %shard_map.73) | data formatting | bytes 1048576

commit v3 on v2

--- a/solution.py
+++ b/solution.py
@@ -9,7 +9,7 @@
 
 SPAN = 128
 GROUP = 2
-TILES = 4
+TILES = 2
 PIECES = 2
 MESH = pl.DeviceIdType.MESH
 F32 = jnp.float32
@@ -248,7 +248,7 @@
     for g in range(groups):
         hs = range(g * GROUP, (g + 1) * GROUP)
 
-        ahead = range(0 if g == 0 else (g + 1) * GROUP, min(g + 2, groups) * GROUP)
+        ahead = range(heads if g == 0 else 0)
 
         @pl.when(jnp.logical_and(jnp.logical_not(first), jnp.logical_not(last)))
         def _():

time: 22.9 us -> 22.5 us (0.983)
  Pallas kernels: 21.9 us -> 21.4 us
    pallas_call x1, Pallas kernels: 21.9 us -> 21.4 us  [body(): pl.pallas_call(functools.partial(kernel, n_sp), out_shape=jax.ShapeDtypeS...]
where the time goes in v3:
time: 22.5 us; the launch traced here: 22.2 us
  Pallas kernels  21.4 us (95%)
  local copies, waits for them, and re-layouts  0.8 us (4%)
    pallas_call x1, Pallas kernels, body(): pl.pallas_call(functools.partial(kernel, n_sp), out_shape=jax.ShapeDtypeS...  21.4 us
    unnamed x1, local copies, waits for them, and re-layouts  0.8 us

profile of v3, /device:TPU:27, one launch (start us, length us, event | category | flops | bytes accessed | tf_op | source)
XLA Modules:
  0.0 22.2 jit_solution(5262457887012492627)
XLA Ops:
  0.0 21.4 %shard_map.73 = bf16[128,2048]{1,0:T(8,128)(2,1)S(1)} custom-call(bf16[256,1024]{1,0:T(8,128)(2,1)} %p_hbm.1, bf16[256,1024]{1,0:T(8,128)(2,1)} %r_hbm.1, bf16[256,1024]{1,0:T(8,128)(2,1)} %v_hbm.1, f32[8,256]{1,0:T(8,128)} %bitcast.3, f32[1,1024]{1,0:T(1,128)} %bitcast.4, f32[1,128]{1,0:T(1,128)} %bitcast.5, bf16[1024,2048]{1,0:T(8,128)(2,1)} %w_hbm.1), custom_call_target="tpu_custom_call" | custom-call | tf_op jit(solution)/shard_map/pallas_call | solution.py:316
  21.4 0.8 %copy.9 = bf16[128,2048]{1,0:T(8,128)(2,1)} copy(bf16[128,2048]{1,0:T(8,128)(2,1)S(1)} %shard_map.73) | data formatting | bytes 1048576
